TPU v7x, 32 devices: a whole 2x2x4 slice. The times are simulated.
32 devices in a mesh: sp: 8 (over z, core), tp: 4 (over y, x).
Axes of the slice: x: 2, y: 2, z: 4, core: 2. Of those that a mesh axis runs over, the one named last changes fastest.
Arguments:
- tokens: bfloat16 [2048, 1024], P('sp', 'tp'), may hold values from -6 to 6
- norm_gain: bfloat16 [2, 1024], P(None, 'tp'), may hold values from 0.099609375 to 1.8984375
- query_weight: bfloat16 [2, 1024, 1024], P(None, 'sp', 'tp'), may hold values from -0.1875 to 0.1875
- key_weight: bfloat16 [2, 1024, 1024], P(None, 'sp', 'tp'), may hold values from -0.1875 to 0.1875
- value_weight: bfloat16 [2, 1024, 1024], P(None, 'sp', 'tp'), may hold values from -0.1875 to 0.1875
- output_weight: bfloat16 [2, 1024, 1024], P(None, 'tp', 'sp'), may hold values from -0.5 to 0.5
- offset_bias: float32 [2, 16, 15, 31], P(None, 'tp'), may hold values from -4 to 4
Outputs:
- mixed: bfloat16 [2048, 1024], P('sp', 'tp')
All inputs are finite; a program needn't handle non-finite values.
Results may differ from a plain program's by a relative error of at most 0.03.
Values may be sent and summed in bfloat16 or wider, within the bound.
A program may use at most 64 MiB of HBM per device.

v0:
```python
import jax
import jax.numpy as jnp
from jax import lax
from jax.sharding import PartitionSpec as P

HEAD_DIM = 64
WIN_H = 8
WIN_W = 16
ROWS_DEV = 4
COLS = 64
D = 1024
norm_eps = 1e-06


def folded(value, axis, dim, update, carry):
    whole = jax.tree.map(lambda part: lax.all_gather(part, axis, axis=dim, tiled=True), value)
    return update(carry, whole, jnp.int32(0))


def extended(block, sides, width, periodic):
    for axis, dim in sides:
        count = lax.axis_size(axis)
        forward = [(i, i + 1) for i in range(count - 1)]
        if periodic:
            forward.append((count - 1, 0))
        backward = [(target, source) for source, target in forward]
        low = lax.ppermute(
            lax.slice_in_dim(block, block.shape[dim] - width, None, axis=dim), axis, forward
        )
        high = lax.ppermute(lax.slice_in_dim(block, 0, width, axis=dim), axis, backward)
        block = jnp.concatenate([low, block, high], axis=dim)
    return block


def own_rows(portion, rows, axis):
    count = rows * lax.axis_size(axis)
    sent = portion(jnp.int32(0), count).astype(jnp.bfloat16)
    return lax.psum_scatter(sent, axis, scatter_dimension=0, tiled=True).astype(jnp.float32)


def attend(query, padded, table, base, total_rows):
    heads = table.shape[0]
    local_width = heads * HEAD_DIM
    half = WIN_H // 2
    span_rows = ROWS_DEV + WIN_H
    glob = base + jnp.arange(ROWS_DEV, dtype=jnp.int32)
    first = jnp.clip(glob - half, 0, total_rows - WIN_H).astype(jnp.int32)
    local_first = first - base + half
    padded_row = jnp.arange(span_rows, dtype=jnp.int32)
    row_inside = (padded_row[None, :] >= local_first[:, None]) & (
        padded_row[None, :] < local_first[:, None] + WIN_H
    )
    row_offset = padded_row[None, :] + base - half - glob[:, None] + (WIN_H - 1)
    row_codes = jnp.arange(2 * WIN_H - 1, dtype=jnp.int32)
    row_onehot = (row_offset[:, :, None] == row_codes[None, None, :]).astype(jnp.float32)
    column = jnp.arange(COLS, dtype=jnp.int32)
    col_start = jnp.clip(column - WIN_W // 2, 0, COLS - WIN_W).astype(jnp.int32)
    col_inside = (column[None, :] >= col_start[:, None]) & (
        column[None, :] < col_start[:, None] + WIN_W
    )
    col_offset = column[None, :] - column[:, None] + (WIN_W - 1)
    col_codes = jnp.arange(2 * WIN_W - 1, dtype=jnp.int32)
    col_onehot = (col_offset[:, :, None] == col_codes[None, None, :]).astype(jnp.float32)
    bias = jnp.einsum(
        "hab,ria,qkb->rhqik", table, row_onehot, col_onehot, precision=lax.Precision.HIGHEST
    )
    inside = row_inside[:, None, None, :, None] & col_inside[None, None, :, None, :]
    keys = padded[:, :, :local_width].reshape(span_rows, COLS, heads, HEAD_DIM)
    values = padded[:, :, local_width:].reshape(span_rows, COLS, heads, HEAD_DIM)
    grid_query = query.reshape(ROWS_DEV, COLS, heads, HEAD_DIM)
    score = jnp.einsum(
        "rqhd,ikhd->rhqik", grid_query, keys, preferred_element_type=jnp.float32
    ) * HEAD_DIM ** (-0.5)
    score = jnp.where(inside, score + bias, -1e30)
    flat = score.reshape(ROWS_DEV, heads, COLS, span_rows * COLS)
    weights = jax.nn.softmax(flat, axis=-1).reshape(score.shape).astype(jnp.bfloat16)
    out = jnp.einsum(
        "rhqik,ikhd->rqhd", weights, values, preferred_element_type=jnp.float32
    ).astype(jnp.bfloat16)
    return out.reshape(ROWS_DEV * COLS, local_width)


def body(tokens, norm_gain, query_weight, key_weight, value_weight, output_weight, offset_bias):
    layers = query_weight.shape[0]
    local_width = query_weight.shape[2]
    feature_rows = tokens.shape[1]
    token_count = tokens.shape[0]
    half = WIN_H // 2
    base = lax.axis_index("sp") * ROWS_DEV
    total_rows = ROWS_DEV * lax.axis_size("sp")
    every = (
        lax.all_gather(query_weight, "sp", axis=1, tiled=True),
        lax.all_gather(key_weight, "sp", axis=1, tiled=True),
        lax.all_gather(value_weight, "sp", axis=1, tiled=True),
        lax.all_gather(output_weight, "sp", axis=2, tiled=True),
    )
    current = tokens
    for layer in range(layers):
        query_full = every[0][layer]
        key_full = every[1][layer]
        value_full = every[2][layer]
        output_full = every[3][layer]
        stacked = jnp.concatenate([query_full, key_full, value_full], axis=1)
        floats = current.astype(jnp.float32)
        squares = lax.psum(jnp.sum(floats * floats, axis=1), "tp")
        factor = lax.rsqrt(squares / D + norm_eps)
        normed = (floats * factor[:, None] * norm_gain[layer].astype(jnp.float32)).astype(
            jnp.bfloat16
        )
        table = offset_bias[layer].astype(jnp.float32)

        def project(carry, piece, start):
            weight_rows = lax.dynamic_slice_in_dim(stacked, start, piece.shape[1], 0)
            return carry + jnp.dot(piece, weight_rows, preferred_element_type=jnp.float32)

        projected = folded(
            normed, "tp", 1, project, jnp.zeros((token_count, 3 * local_width), jnp.float32)
        ).astype(jnp.bfloat16)
        query = projected[:, :local_width]
        pair = projected[:, local_width:].reshape(ROWS_DEV, COLS, 2 * local_width)
        padded = extended(pair, (("sp", 0),), half, False)
        attended = attend(query, padded, table, base, total_rows)

        def project_out(start, count):
            weight_cols = lax.dynamic_slice_in_dim(output_full, start, count, 1)
            return lax.dot_general(
                weight_cols, attended, (((0,), (1,)), ((), ())), preferred_element_type=jnp.float32
            )

        summed = own_rows(project_out, feature_rows, "tp")
        current = summed.T.astype(jnp.bfloat16)
    return current


def solution(mesh):
    in_specs = (
        P("sp", "tp"),
        P(None, "tp"),
        P(None, "sp", "tp"),
        P(None, "sp", "tp"),
        P(None, "sp", "tp"),
        P(None, "tp", "sp"),
        P(None, "tp", None, None),
    )
    out_specs = P("sp", "tp")
    return jax.shard_map(body, mesh=mesh, in_specs=in_specs, out_specs=out_specs, check_vma=False)
```

profile of v0, /device:TPU:0, one launch (start us, length us, event | category | flops | bytes accessed | tf_op | source)
XLA Modules:
  0.0 223.2 jit_solution(17769417152890954253)
XLA Ops:
  11.2 11.4 %psum.14 = f32[256]{0:T(256)S(1)} all-reduce(f32[256]{0:T(256)S(1)} %fusion.59), channel_id=1, replica_groups=mesh['sp'=8,'tp'=4] {'tp'}, use_global_device_ids=true, to_apply=%region_1.0 | all-reduce | flops 256 | bytes 2048 | tf_op jit(solution)/shard_map/psum | solution.py:105
  23.6 11.2 %all_gather.18 = bf16[256,1024]{1,0:T(8,128)(2,1)S(1)} all-gather(bf16[256,256]{1,0:T(8,128)(2,1)S(1)} %fusion.61), channel_id=1, replica_groups=mesh['sp'=8,'tp'=4] {'tp'}, dimensions={1}, use_global_device_ids=true | all-gather | bytes 655360 | tf_op jit(solution)/shard_map/all_gather | solution.py:16
  35.0 1.4 fusion.79
  37.5 5.7 %fusion.10 = f32[64,64,4,4,12]{1,4,3,2,0:T(8,128)} fusion(f32[64,64,4,15]{1,3,2,0:T(8,128)S(1)} %fusion.53, s32[4,12]{1,0:T(4,128)S(1)} %subtract_add_fusion.1), kind=kOutput, calls=%fused_computation.16 | convolution fusion | flops 141558480 | bytes 4128960 | tf_op jit(solution)/shard_map/hab,ria,qkb->rhqik/dot_general | solution.py:64
  43.2 2.1 slice_bitcast_fusion.2
  45.2 12.2 %all-gather.5.cloned.1.call-done = bf16[2,1024,256]{2,1,0:T(8,128)(2,1)} async-done(((bf16[2,128,256]{2,1,0:T(8,128)(2,1)}), bf16[2,1024,256]{2,1,0:T(8,128)(2,1)}) %all-gather.5.cloned.1.call-update) | async-done | bytes 1048592 | tf_op jit(solution)/shard_map/all_gather | solution.py:92
  57.4 2.1 slice_bitcast_fusion.4
  59.5 21.4 %all-gather.7.cloned.1.call-done = bf16[2,1024,256]{2,1,0:T(8,128)(2,1)} async-done(((bf16[2,128,256]{2,1,0:T(8,128)(2,1)}), bf16[2,1024,256]{2,1,0:T(8,128)(2,1)}) %all-gather.7.cloned.1.call-update) | async-done | bytes 1048592 | tf_op jit(solution)/shard_map/all_gather | solution.py:93
  80.9 2.1 slice_bitcast_fusion.3
  83.6 2.1 collective-permute-start
  85.7 1.3 collective-permute-start.1
  87.0 9.8 %copy.30 = f32[64,64,4,4,12]{0,1,3,4,2:T(8,128)} copy(f32[64,64,4,4,12]{1,4,3,2,0:T(8,128)} %fusion.10) | data formatting | bytes 6291456 | tf_op jit(solution)/shard_map/hab,ria,qkb->rhqik/dot_general | solution.py:64
  98.1 4.5 %fusion.80 = (f32[4,4,64]{2,0,1:T(4,128)S(1)}, f32[4,4,64,12,64]{2,4,0,3,1:T(8,128)S(1)}) fusion(f32[64,64,4,4,12]{0,1,3,4,2:T(8,128)} %copy.30, bf16[4,64,4,64,1]{3,2,1,0,4:T(4,128)(2,1)S(1)} %bitcast.99, bf16[12,64,4,64,1]{3,2,1,0,4:T(4,128)(2,1)S(1)} %bitcast.97, pred[4,64,12,64]{1,3,0,2:T(8,128)(4,1)S(1)} %broadcast_and_fusion), kind=kOutput, calls=%fused_computation.106 | convolution fusion | flops 103808000 | bytes 7016448 | tf_op jit(solution)/shard_map/rqhd,ikhd->rhqik/dot_general | solution.py:71
  106.6 2.1 fusion.36
  108.8 1.8 fusion.51
  110.6 23.9 %reduce-scatter.3.cloned.1.call-done = bf16[256,256]{0,1:T(8,128)(2,1)} async-done(((bf16[1024,256]{0,1:T(8,128)(2,1)}), bf16[256,256]{0,1:T(8,128)(2,1)}) %reduce-scatter.3.cloned.1.call-update) | async-done | bytes 131088 | tf_op jit(solution)/shard_map/reduce_scatter | solution.py:38
  135.6 9.1 %psum.15 = f32[256]{0:T(256)S(1)} all-reduce(f32[256]{0:T(256)S(1)} %fusion.62), channel_id=1, replica_groups=mesh['sp'=8,'tp'=4] {'tp'}, use_global_device_ids=true, to_apply=%region_6.7 | all-reduce | flops 256 | bytes 2048 | tf_op jit(solution)/shard_map/psum | solution.py:105
  145.7 12.1 %all_gather.23 = bf16[256,1024]{1,0:T(8,128)(2,1)S(1)} all-gather(bf16[256,256]{1,0:T(8,128)(2,1)S(1)} %fusion.67), channel_id=1, replica_groups=mesh['sp'=8,'tp'=4] {'tp'}, dimensions={1}, use_global_device_ids=true | all-gather | bytes 655360 | tf_op jit(solution)/shard_map/all_gather | solution.py:16
  157.8 2.0 fusion.24
  159.8 1.3 collective-permute-start.2
  162.4 5.7 %fusion.8 = f32[64,64,4,4,12]{1,4,3,2,0:T(8,128)} fusion(f32[64,64,4,15]{1,3,2,0:T(8,128)S(1)} %fusion.51, s32[4,12]{1,0:T(4,128)S(1)} %subtract_add_fusion.1), kind=kOutput, calls=%fused_computation.14 | convolution fusion | flops 141558480 | bytes 4128960 | tf_op jit(solution)/shard_map/hab,ria,qkb->rhqik/dot_general | solution.py:64
  168.1 9.8 %copy.38 = f32[64,64,4,4,12]{0,1,3,4,2:T(8,128)} copy(f32[64,64,4,4,12]{1,4,3,2,0:T(8,128)} %fusion.8) | data formatting | bytes 6291456 | tf_op jit(solution)/shard_map/hab,ria,qkb->rhqik/dot_general | solution.py:64
  179.8 4.5 %fusion.81 = (f32[4,4,64]{2,0,1:T(4,128)S(1)}, f32[4,4,64,12,64]{2,4,0,3,1:T(8,128)S(1)}) fusion(f32[64,64,4,4,12]{0,1,3,4,2:T(8,128)} %copy.38, bf16[4,64,4,64,1]{3,2,1,0,4:T(4,128)(2,1)S(1)} %bitcast.98, bf16[12,64,4,64,1]{3,2,1,0,4:T(4,128)(2,1)S(1)} %bitcast.96, pred[4,64,12,64]{1,3,0,2:T(8,128)(4,1)S(1)} %broadcast_and_fusion), kind=kOutput, calls=%fused_computation.107 | convolution fusion | flops 103808000 | bytes 7016448 | tf_op jit(solution)/shard_map/rqhd,ikhd->rhqik/dot_general | solution.py:71
  188.1 28.2 %reduce-scatter.5.cloned.1.call-done = bf16[256,256]{0,1:T(8,128)(2,1)} async-done(((bf16[1024,256]{0,1:T(8,128)(2,1)}), bf16[256,256]{0,1:T(8,128)(2,1)}) %reduce-scatter.5.cloned.1.call-update) | async-done | bytes 131088 | tf_op jit(solution)/shard_map/reduce_scatter | solution.py:38
  (63 shorter events, 21.7 us)
Async XLA Ops:
  6.5 36.6 %all-gather.9.cloned.1.call-start = ((), (), s32[]{:S(2)}) async-start(), calls=%async_computation.4 | async-start | bytes 1179648 | tf_op jit(solution)/shard_map/all_gather | solution.py:94
  7.3 50.2 %all-gather.5.cloned.1.call-start = ((), (), s32[]{:S(2)}) async-start(), calls=%async_computation.2 | async-start | bytes 1179648 | tf_op jit(solution)/shard_map/all_gather | solution.py:92
  8.0 72.9 %all-gather.7.cloned.1.call-start = ((), (), s32[]{:S(2)}) async-start(), calls=%async_computation.3 | async-start | bytes 1179648 | tf_op jit(solution)/shard_map/all_gather | solution.py:93
  8.7 97.9 %all-gather.11.cloned.1.call-start = ((), (), s32[]{:S(2)}) async-start(), calls=%async_computation.5 | async-start | bytes 1179648 | tf_op jit(solution)/shard_map/all_gather | solution.py:95
  9.3 125.2 %reduce-scatter.3.cloned.1.call-start = ((), (), s32[]{:S(2)}) async-start(), calls=%async_computation.6 | async-start | bytes 655360 | tf_op jit(solution)/shard_map/reduce_scatter | solution.py:38
  83.6 13.7 %collective-permute-start = (bf16[4,64,512]{2,1,0:T(8,128)(2,1)S(1)}, bf16[4,64,512]{2,1,0:T(8,128)(2,1)S(1)}, u32[]{:S(2)}, u32[]{:S(2)}) collective-permute-start(bf16[4,64,512]{2,1,0:T(8,128)(2,1)S(1)} %bitcast.100), channel_id=1, source_target_pairs={{0,4},{4,8},{8,12},{12,16},{16,20},{20,24},{24,28},{1,5},{5,9},{9,... | collective-permute-start | bytes 786440 | tf_op jit(solution)/shard_map/ppermute | solution.py:27
  85.7 11.6 %collective-permute-start.1 = (bf16[4,64,512]{2,1,0:T(8,128)(2,1)S(1)}, bf16[4,64,512]{2,1,0:T(8,128)(2,1)S(1)}, u32[]{:S(2)}, u32[]{:S(2)}) collective-permute-start(bf16[4,64,512]{2,1,0:T(8,128)(2,1)S(1)} %bitcast.101), channel_id=1, source_target_pairs={{4,0},{8,4},{12,8},{16,12},{20,16},{24,20},{28,24},{5,1},{9,5},{13... | collective-permute-start | bytes 786440 | tf_op jit(solution)/shard_map/ppermute | solution.py:30
  108.8 107.6 %reduce-scatter.5.cloned.1.call-start = ((), (), s32[]{:S(2)}) async-start(), calls=%async_computation.7 | async-start | bytes 655360 | tf_op jit(solution)/shard_map/reduce_scatter | solution.py:38
  159.8 18.2 %collective-permute-start.2 = (bf16[4,64,512]{2,1,0:T(8,128)(2,1)S(1)}, bf16[4,64,512]{2,1,0:T(8,128)(2,1)S(1)}, u32[]{:S(2)}, u32[]{:S(2)}) collective-permute-start(bf16[4,64,512]{2,1,0:T(8,128)(2,1)S(1)} %bitcast.103), channel_id=1, source_target_pairs={{0,4},{4,8},{8,12},{12,16},{16,20},{20,24},{24,28},{1,5},{5,9},{9,... | collective-permute-start | bytes 786440 | tf_op jit(solution)/shard_map/ppermute | solution.py:27
  161.1 16.9 %collective-permute-start.3 = (bf16[4,64,512]{2,1,0:T(8,128)(2,1)S(1)}, bf16[4,64,512]{2,1,0:T(8,128)(2,1)}, u32[]{:S(2)}, u32[]{:S(2)}) collective-permute-start(bf16[4,64,512]{2,1,0:T(8,128)(2,1)S(1)} %bitcast.104), channel_id=1, source_target_pairs={{4,0},{8,4},{12,8},{16,12},{20,16},{24,20},{28,24},{5,1},{9,5},{13... | collective-permute-start | bytes 786440 | tf_op jit(solution)/shard_map/ppermute | solution.py:30
  185.4 1.6 copy-start
Sparse Core Ops, SparseCore 0:
  8.9 24.9 all-gather.8
  35.5 21.8 all-gather.4
  59.0 21.8 all-gather.6
  82.3 24.2 all-gather.10
  109.3 25.2 reduce-scatter.2
  188.2 28.0 reduce-scatter.4
where the time goes:
time: 224 us; the launch traced here: 223 us
  waiting for transfers between devices  89.7 us (40%)
  blocking collectives  43.8 us (20%)
  matrix products  31.3 us (14%)
  local copies, waits for them, and re-layouts  29.8 us (13%)
  between operations  13.8 us (6%)
  other arithmetic  8.54 us (4%)
  starting transfers between devices  6.23 us (3%)
    reduce_scatter x2, waiting for transfers between devices, own_rows(): lax.psum_scatter(sent, axis, scatter_dimension=0, tiled=True)  52.2 us
    all_gather x2, blocking collectives, folded(): lax.all_gather(part, axis, axis=dim, tiled=True)  23.3 us
    all_gather x1, waiting for transfers between devices, body(): lax.all_gather(key_weight, 'sp', axis=1, tiled=True)  21.4 us
    psum x2, blocking collectives, body(): squares = lax.psum(jnp.sum(floats * floats, axis=1), 'tp')  20.5 us
    dot_general x2, local copies, waits for them, and re-layouts, attend(): jnp.einsum('hab,ria,qkb->rhqik', table, row_onehot, col_onehot, precision...  19.6 us
    dot_general x4, matrix products, attend(): jnp.einsum('hab,ria,qkb->rhqik', table, row_onehot, col_onehot, precision...  14.1 us
    all_gather x1, waiting for transfers between devices, body(): lax.all_gather(query_weight, 'sp', axis=1, tiled=True)  12.2 us
    dot_general x2, matrix products, attend(): jnp.einsum('rqhd,ikhd->rhqik', grid_query, keys, preferred_element_type=j...  9.06 us
  transfers between devices with their start and end apart: 10, of which 5 were waited for; matrix products, arithmetic and copies ran while one was open for 24% of the time, Pallas kernels for 0%

commit v1 on v0

--- a/solution.py
+++ b/solution.py
@@ -2,6 +2,7 @@
 import jax.numpy as jnp
 from jax import lax
 from jax.sharding import PartitionSpec as P
+from jax.lax import all_gather
 
 HEAD_DIM = 64
 WIN_H = 8
@@ -102,7 +103,8 @@
         output_full = every[3][layer]
         stacked = jnp.concatenate([query_full, key_full, value_full], axis=1)
         floats = current.astype(jnp.float32)
-        squares = lax.psum(jnp.sum(floats * floats, axis=1), "tp")
+        unit = jnp.sum(floats * floats, axis=1)
+        squares = all_gather(unit, "tp").sum(axis=0)
         factor = lax.rsqrt(squares / D + norm_eps)
         normed = (floats * factor[:, None] * norm_gain[layer].astype(jnp.float32)).astype(
             jnp.bfloat16

time: 224 us -> 222 us (level)
  blocking collectives: 43.8 us -> 41.1 us
  waiting for transfers between devices: 89.7 us -> 92.1 us
    psum x2 -> x0, blocking collectives: 20.5 us -> none  [body(): squares = lax.psum(jnp.sum(floats * floats, axis=1), 'tp')]
    all_gather x0 -> x2, blocking collectives: none -> 17.6 us  [body(): squares = all_gather(unit, 'tp').sum(axis=0)]
  transfers between devices with their start and end apart: 10 -> 10, of which waited for: 5 -> 5; matrix products, arithmetic and copies ran while one was open for 24% -> 23% of each run, Pallas kernels for 0% -> 0%
where the time goes in v1:
time: 222 us; the launch traced here: 221 us
  waiting for transfers between devices  92.1 us (41%)
  blocking collectives  41.1 us (19%)
  matrix products  30.4 us (14%)
  local copies, waits for them, and re-layouts  29.2 us (13%)
  between operations  13.8 us (6%)
  other arithmetic  8.45 us (4%)
  starting transfers between devices  6.23 us (3%)
    reduce_scatter x2, waiting for transfers between devices, own_rows(): lax.psum_scatter(sent, axis, scatter_dimension=0, tiled=True)  52.9 us
    all_gather x2, blocking collectives, folded(): lax.all_gather(part, axis, axis=dim, tiled=True)  23.5 us
    all_gather x1, waiting for transfers between devices, body(): lax.all_gather(key_weight, 'sp', axis=1, tiled=True)  21.4 us
    dot_general x2, local copies, waits for them, and re-layouts, attend(): jnp.einsum('hab,ria,qkb->rhqik', table, row_onehot, col_onehot, precision...  19.6 us
    all_gather x2, blocking collectives, body(): squares = all_gather(unit, 'tp').sum(axis=0)  17.6 us
    all_gather x1, waiting for transfers between devices, body(): lax.all_gather(query_weight, 'sp', axis=1, tiled=True)  13.8 us
    dot_general x4, matrix products, attend(): jnp.einsum('hab,ria,qkb->rhqik', table, row_onehot, col_onehot, precision...  13.3 us
    dot_general x2, matrix products, attend(): jnp.einsum('rqhd,ikhd->rhqik', grid_query, keys, preferred_element_type=j...  9.06 us
  transfers between devices with their start and end apart: 10, of which 5 were waited for; matrix products, arithmetic and copies ran while one was open for 23% of the time, Pallas kernels for 0%

profile of v1, /device:TPU:0, one launch (start us, length us, event | category | flops | bytes accessed | tf_op | source)
XLA Modules:
  0.0 221.4 jit_solution(12100841044575629911)
XLA Ops:
  11.2 9.6 %all-gather.2 = f32[4,1,256]{2,1,0:T(1,128)S(1)} all-gather(f32[1,1,256]{2,1,0:T(1,128)S(1)} %bitcast.113), channel_id=2, replica_groups=mesh['sp'=8,'tp'=4] {'tp'}, dimensions={0}, use_global_device_ids=true | all-gather | bytes 5120 | tf_op jit(solution)/shard_map/all_gather | solution.py:107
  21.8 12.1 %all_gather.32 = bf16[256,1024]{1,0:T(8,128)(2,1)S(1)} all-gather(bf16[256,256]{1,0:T(8,128)(2,1)S(1)} %fusion.63), channel_id=1, replica_groups=mesh['sp'=8,'tp'=4] {'tp'}, dimensions={1}, use_global_device_ids=true | all-gather | bytes 655360 | tf_op jit(solution)/shard_map/all_gather | solution.py:17
  35.8 5.7 %fusion.10 = f32[64,64,4,4,12]{1,4,3,2,0:T(8,128)} fusion(f32[64,64,4,15]{1,3,2,0:T(8,128)S(1)} %fusion.53, s32[4,12]{1,0:T(4,128)S(1)} %subtract_add_fusion.1), kind=kOutput, calls=%fused_computation.16 | convolution fusion | flops 141558480 | bytes 4128960 | tf_op jit(solution)/shard_map/hab,ria,qkb->rhqik/dot_general | solution.py:65
  41.5 2.1 slice_bitcast_fusion.2
  43.6 13.8 %all-gather.9.cloned.1.call-done = bf16[2,1024,256]{2,1,0:T(8,128)(2,1)} async-done(((bf16[2,128,256]{2,1,0:T(8,128)(2,1)}), bf16[2,1024,256]{2,1,0:T(8,128)(2,1)}) %all-gather.9.cloned.1.call-update) | async-done | bytes 1048592 | tf_op jit(solution)/shard_map/all_gather | solution.py:93
  57.4 2.1 slice_bitcast_fusion.4
  59.5 21.4 %all-gather.11.cloned.1.call-done = bf16[2,1024,256]{2,1,0:T(8,128)(2,1)} async-done(((bf16[2,128,256]{2,1,0:T(8,128)(2,1)}), bf16[2,1024,256]{2,1,0:T(8,128)(2,1)}) %all-gather.11.cloned.1.call-update) | async-done | bytes 1048592 | tf_op jit(solution)/shard_map/all_gather | solution.py:94
  80.9 2.1 slice_bitcast_fusion.3
  83.6 2.1 collective-permute-start
  85.7 1.3 collective-permute-start.1
  87.0 9.8 %copy.29 = f32[64,64,4,4,12]{0,1,3,4,2:T(8,128)} copy(f32[64,64,4,4,12]{1,4,3,2,0:T(8,128)} %fusion.10) | data formatting | bytes 6291456 | tf_op jit(solution)/shard_map/hab,ria,qkb->rhqik/dot_general | solution.py:65
  98.1 4.5 %fusion.82 = (f32[4,4,64]{2,0,1:T(4,128)S(1)}, f32[4,4,64,12,64]{2,4,0,3,1:T(8,128)S(1)}) fusion(f32[64,64,4,4,12]{0,1,3,4,2:T(8,128)} %copy.29, bf16[4,64,4,64,1]{3,2,1,0,4:T(4,128)(2,1)S(1)} %bitcast.104, bf16[12,64,4,64,1]{3,2,1,0,4:T(4,128)(2,1)S(1)} %bitcast.102, pred[4,64,12,64]{1,3,0,2:T(8,128)(4,1)S(1)} %broadcast_and_fusion), kind=kOutput, calls=%fused_computation.106 | convolution fusion | flops 103808000 | bytes 7016448 | tf_op jit(solution)/shard_map/rqhd,ikhd->rhqik/dot_general | solution.py:72
  105.3 1.3 all-gather.15.cloned.1.call-done
  106.6 2.1 fusion.36
  109.8 24.7 %reduce-scatter.3.cloned.1.call-done = bf16[256,256]{0,1:T(8,128)(2,1)} async-done(((bf16[1024,256]{0,1:T(8,128)(2,1)}), bf16[256,256]{0,1:T(8,128)(2,1)}) %reduce-scatter.3.cloned.1.call-update) | async-done | bytes 131088 | tf_op jit(solution)/shard_map/reduce_scatter | solution.py:39
  135.5 8.0 %all-gather.3 = f32[4,1,256]{2,1,0:T(1,128)S(1)} all-gather(f32[1,1,256]{2,1,0:T(1,128)S(1)} %bitcast.114), channel_id=3, replica_groups=mesh['sp'=8,'tp'=4] {'tp'}, dimensions={0}, use_global_device_ids=true | all-gather | bytes 5120 | tf_op jit(solution)/shard_map/all_gather | solution.py:107
  144.6 11.4 %all_gather.39 = bf16[256,1024]{1,0:T(8,128)(2,1)S(1)} all-gather(bf16[256,256]{1,0:T(8,128)(2,1)S(1)} %fusion.69), channel_id=1, replica_groups=mesh['sp'=8,'tp'=4] {'tp'}, dimensions={1}, use_global_device_ids=true | all-gather | bytes 655360 | tf_op jit(solution)/shard_map/all_gather | solution.py:17
  156.0 2.0 fusion.24
  158.0 1.3 collective-permute-start.2
  159.3 1.3 collective-permute-start.3
  160.6 5.7 %fusion.8 = f32[64,64,4,4,12]{1,4,3,2,0:T(8,128)} fusion(f32[64,64,4,15]{1,3,2,0:T(8,128)S(1)} %fusion.51, s32[4,12]{1,0:T(4,128)S(1)} %subtract_add_fusion.1), kind=kOutput, calls=%fused_computation.14 | convolution fusion | flops 141558480 | bytes 4128960 | tf_op jit(solution)/shard_map/hab,ria,qkb->rhqik/dot_general | solution.py:65
  166.2 9.8 %copy.36 = f32[64,64,4,4,12]{0,1,3,4,2:T(8,128)} copy(f32[64,64,4,4,12]{1,4,3,2,0:T(8,128)} %fusion.8) | data formatting | bytes 6291456 | tf_op jit(solution)/shard_map/hab,ria,qkb->rhqik/dot_general | solution.py:65
  178.0 4.5 %fusion.83 = (f32[4,4,64]{2,0,1:T(4,128)S(1)}, f32[4,4,64,12,64]{2,4,0,3,1:T(8,128)S(1)}) fusion(f32[64,64,4,4,12]{0,1,3,4,2:T(8,128)} %copy.36, bf16[4,64,4,64,1]{3,2,1,0,4:T(4,128)(2,1)S(1)} %bitcast.103, bf16[12,64,4,64,1]{3,2,1,0,4:T(4,128)(2,1)S(1)} %bitcast.101, pred[4,64,12,64]{1,3,0,2:T(8,128)(4,1)S(1)} %broadcast_and_fusion), kind=kOutput, calls=%fused_computation.107 | convolution fusion | flops 103808000 | bytes 7016448 | tf_op jit(solution)/shard_map/rqhd,ikhd->rhqik/dot_general | solution.py:72
  186.3 28.2 %reduce-scatter.5.cloned.1.call-done = bf16[256,256]{0,1:T(8,128)(2,1)} async-done(((bf16[1024,256]{0,1:T(8,128)(2,1)}), bf16[256,256]{0,1:T(8,128)(2,1)}) %reduce-scatter.5.cloned.1.call-update) | async-done | bytes 131088 | tf_op jit(solution)/shard_map/reduce_scatter | solution.py:39
  (64 shorter events, 20.7 us)
Async XLA Ops:
  6.5 34.9 %all-gather.13.cloned.1.call-start = ((), (), s32[]{:S(2)}) async-start(), calls=%async_computation.4 | async-start | bytes 1179648 | tf_op jit(solution)/shard_map/all_gather | solution.py:95
  7.3 50.2 %all-gather.9.cloned.1.call-start = ((), (), s32[]{:S(2)}) async-start(), calls=%async_computation.2 | async-start | bytes 1179648 | tf_op jit(solution)/shard_map/all_gather | solution.py:93
  8.0 72.9 %all-gather.11.cloned.1.call-start = ((), (), s32[]{:S(2)}) async-start(), calls=%async_computation.3 | async-start | bytes 1179648 | tf_op jit(solution)/shard_map/all_gather | solution.py:94
  8.7 97.9 %all-gather.15.cloned.1.call-start = ((), (), s32[]{:S(2)}) async-start(), calls=%async_computation.5 | async-start | bytes 1179648 | tf_op jit(solution)/shard_map/all_gather | solution.py:96
  9.3 125.2 %reduce-scatter.3.cloned.1.call-start = ((), (), s32[]{:S(2)}) async-start(), calls=%async_computation.6 | async-start | bytes 655360 | tf_op jit(solution)/shard_map/reduce_scatter | solution.py:39
  83.6 13.7 %collective-permute-start = (bf16[4,64,512]{2,1,0:T(8,128)(2,1)S(1)}, bf16[4,64,512]{2,1,0:T(8,128)(2,1)S(1)}, u32[]{:S(2)}, u32[]{:S(2)}) collective-permute-start(bf16[4,64,512]{2,1,0:T(8,128)(2,1)S(1)} %bitcast.105), channel_id=1, source_target_pairs={{0,4},{4,8},{8,12},{12,16},{16,20},{20,24},{24,28},{1,5},{5,9},{9,... | collective-permute-start | bytes 786440 | tf_op jit(solution)/shard_map/ppermute | solution.py:28
  85.7 11.6 %collective-permute-start.1 = (bf16[4,64,512]{2,1,0:T(8,128)(2,1)S(1)}, bf16[4,64,512]{2,1,0:T(8,128)(2,1)S(1)}, u32[]{:S(2)}, u32[]{:S(2)}) collective-permute-start(bf16[4,64,512]{2,1,0:T(8,128)(2,1)S(1)} %bitcast.106), channel_id=1, source_target_pairs={{4,0},{8,4},{12,8},{16,12},{20,16},{24,20},{28,24},{5,1},{9,5},{13... | collective-permute-start | bytes 786440 | tf_op jit(solution)/shard_map/ppermute | solution.py:31
  108.8 105.7 %reduce-scatter.5.cloned.1.call-start = ((), (), s32[]{:S(2)}) async-start(), calls=%async_computation.7 | async-start | bytes 655360 | tf_op jit(solution)/shard_map/reduce_scatter | solution.py:39
  158.0 18.2 %collective-permute-start.2 = (bf16[4,64,512]{2,1,0:T(8,128)(2,1)S(1)}, bf16[4,64,512]{2,1,0:T(8,128)(2,1)S(1)}, u32[]{:S(2)}, u32[]{:S(2)}) collective-permute-start(bf16[4,64,512]{2,1,0:T(8,128)(2,1)S(1)} %bitcast.108), channel_id=1, source_target_pairs={{0,4},{4,8},{8,12},{12,16},{16,20},{20,24},{24,28},{1,5},{5,9},{9,... | collective-permute-start | bytes 786440 | tf_op jit(solution)/shard_map/ppermute | solution.py:28
  159.3 16.9 %collective-permute-start.3 = (bf16[4,64,512]{2,1,0:T(8,128)(2,1)S(1)}, bf16[4,64,512]{2,1,0:T(8,128)(2,1)}, u32[]{:S(2)}, u32[]{:S(2)}) collective-permute-start(bf16[4,64,512]{2,1,0:T(8,128)(2,1)S(1)} %bitcast.109), channel_id=1, source_target_pairs={{4,0},{8,4},{12,8},{16,12},{20,16},{24,20},{28,24},{5,1},{9,5},{13... | collective-permute-start | bytes 786440 | tf_op jit(solution)/shard_map/ppermute | solution.py:31
  183.5 1.6 copy-start
Sparse Core Ops, SparseCore 0:
  8.9 24.9 all-gather.12
  35.5 21.8 all-gather.8
  59.0 21.8 all-gather.10
  82.3 24.2 all-gather.14
  109.3 25.1 reduce-scatter.2
  186.4 28.0 reduce-scatter.4
